TPU v7x, 32 devices: a whole 2x2x4 slice. The times are simulated.
32 devices in a mesh: kv: 8 (over z, x), tp: 4 (over y, core).
Axes of the slice: x: 2, y: 2, z: 4, core: 2. Of those that a mesh axis runs over, the one named last changes fastest.
Arguments:
- inputs: bfloat16 [2048, 2048], P('kv', 'tp'), may hold values from -6 to 6
- queries: bfloat16 [2048, 2048], P('kv', 'tp'), may hold values from -8 to 8
- key_vectors: bfloat16 [2048, 512], P('kv', 'tp'), may hold values from -8 to 8
- value_rows_by_head: bfloat16 [2048, 512], P('kv', 'tp'), may hold values from -6 to 6
- out_grad: bfloat16 [2048, 2048], P('kv', 'tp'), may hold values from -6 to 6
- chosen: int32 [16, 16], replicated, may hold values from 0 to 31, as said below
Outputs:
- query_grad: bfloat16 [2048, 2048], P('kv', 'tp')
- key_grad: bfloat16 [2048, 512], P('kv', 'tp')
- value_grad: bfloat16 [2048, 512], P('kv', 'tp')
- weight_grad: float32 [2048, 2048], P('kv', 'tp')
Inputs may be any that keep to these rules, and one draw needn't show every extreme that they name: `chosen`: row r holds 16 distinct key-block numbers, among them every key block that intersects query block r. The rows of one device (aligned runs of 2 rows) name at most 2 distinct key blocks that lie on any one other device (aligned runs of 4 key blocks), and exactly 2 at some other device for some devices.
All inputs are finite; a program needn't handle non-finite values.
Results may differ from a plain program's by a relative error of at most 0.015.
The roundings to bfloat16 on the way count: a program that leaves them out, or rounds other values in their place, can miss the bound.
Values may be sent and summed in bfloat16 or wider, within the bound.
A program may use at most 128 MiB of HBM per device.

v0:
```python
import functools

import jax
import jax.numpy as jnp
from jax import lax
from jax.experimental import pallas as pl
from jax.experimental.pallas import tpu as pltpu
from jax.sharding import PartitionSpec as P

HEAD_SIZE = 64
QB = 128
KB = 64
HEADS_PER_KEY = 4
NEG = -1e30
BF16 = jnp.bfloat16
F32 = jnp.float32


def dot_nt(x, y):
    return lax.dot_general(x, y, (((1,), (1,)), ((), ())), preferred_element_type=F32)


def dot_nn(x, y):
    return lax.dot_general(x, y, (((1,), (0,)), ((), ())), preferred_element_type=F32)


def dot_tn(x, y):
    return lax.dot_general(x, y, (((0,), (0,)), ((), ())), preferred_element_type=F32)


def kernel(
    n, tp, a, b,
    sel_ref, x_ref, q_ref, k_ref, v_ref, g_ref,
    dq_ref, dk_ref, dv_ref, w_ref,
    kvst, kvbuf, xst, xbuf, q_s, g_s, s_buf, dp_buf, dq_acc, gst, grecv, own_acc,
    qall, wst, wrecv, w_own,
    kv_send, kv_recv, x_send, x_recv, g_send, g_recv, q_send, q_recv, w_send, w_recv,
):
    me = lax.axis_index("kv")
    t = lax.axis_index("tp")
    alpha = lax.rem(me, a)
    beta = lax.div(me, a)
    rows, cols = k_ref.shape
    heads = cols // HEAD_SIZE
    group = q_ref.shape[1] // cols
    local = rows // QB
    owner = rows // KB
    chunk = local * KB
    own_chunks = rows // chunk
    wide = group * rows
    width = xst.shape[2]
    n_chunk = xst.shape[0]
    gcols = group * HEAD_SIZE
    scale = HEAD_SIZE ** (-0.5)

    def remote(src, dst, send, recv, kv, tpi):
        return pltpu.make_async_remote_copy(
            src_ref=src, dst_ref=dst, send_sem=send, recv_sem=recv,
            device_id=(kv, tpi), device_id_type=pl.DeviceIdType.MESH,
        )

    barrier = pltpu.get_barrier_semaphore()
    for d in range(1, n):
        pl.semaphore_signal(
            barrier, inc=1, device_id=(lax.rem(me + d, n), t), device_id_type=pl.DeviceIdType.MESH
        )
    for d in range(1, tp):
        for m in range(a):
            pl.semaphore_signal(
                barrier, inc=1, device_id=(beta * a + m, lax.rem(t + d, tp)),
                device_id_type=pl.DeviceIdType.MESH,
            )

    def slots(i, j):
        used = []
        for blk in range(owner):
            u = sel_ref[i * local, j * owner + blk]
            for r in range(1, local):
                u = jnp.maximum(u, sel_ref[i * local + r, j * owner + blk])
            used.append(u)
        picks = []
        for p in range(local):
            before = jnp.int32(0)
            one = []
            for blk in range(owner):
                one.append(jnp.where(before == p, used[blk], 0))
                before = before + used[blk]
            picks.append(one)
        return picks

    def stage_kv(i, carry):
        picks = slots(i, me)
        for p in range(local):
            at = slice(p * KB, (p + 1) * KB)
            for ref, first in ((k_ref, 0), (v_ref, cols)):
                out = jnp.zeros((KB, cols), F32)
                for blk in range(owner):
                    rows_of = ref[blk * KB : (blk + 1) * KB, :].astype(F32)
                    out = jnp.where(picks[p][blk] > 0, rows_of, out)
                kvst[i, at, first : first + cols] = out.astype(BF16)
        return carry

    lax.fori_loop(me + 1, n, stage_kv, 0)
    for q in range(n_chunk):
        xst[q] = x_ref[:, q * width : (q + 1) * width]

    pl.semaphore_wait(barrier, n - 1 + (tp - 1) * a)

    def kv_copy(i, j):
        return remote(kvst.at[i], kvbuf.at[j], kv_send.at[i], kv_recv.at[j], i, t)

    def start_kv(i, carry):
        kv_copy(i, me).start()
        return carry

    lax.fori_loop(me + 1, n, start_kv, 0)

    def x_copy(q, tt):
        c = t * n_chunk + q
        return remote(
            xst.at[q], xbuf.at[alpha, lax.div(c, a)], x_send.at[q, tt],
            x_recv.at[alpha, lax.div(c, a)], beta * a + lax.rem(c, a), tt,
        )

    for q in range(n_chunk):
        c = t * n_chunk + q
        for tt in range(tp):
            mine = jnp.logical_and(lax.rem(c, a) == alpha, t == tt)

            @pl.when(jnp.logical_not(mine))
            def _():
                x_copy(q, tt).start()

            @pl.when(mine)
            def _():
                xbuf[alpha, lax.div(c, a)] = x_ref[:, q * width : (q + 1) * width]

    lane = lax.rem(lax.broadcasted_iota(jnp.int32, (1, wide), 1), rows)
    lane_block = lax.div(lane, QB)

    def row_bias(flags):
        vals = [jnp.where(f > 0, F32(0.0), F32(NEG)) for f in flags]
        out = jnp.full((1, wide), vals[0], F32)
        for r in range(1, local):
            out = jnp.where(lane_block == r, vals[r], out)
        return out

    def head_cols(h):
        return slice(h * HEAD_SIZE, (h + 1) * HEAD_SIZE)

    def own_kv(o, h):
        at = slice(o * chunk, (o + 1) * chunk)
        return k_ref[at, head_cols(h)], v_ref[at, head_cols(h)]

    def far_k(j, h):
        return kvbuf[j, :, head_cols(h)]

    def far_v(j, h):
        return kvbuf[j, :, cols + h * HEAD_SIZE : cols + (h + 1) * HEAD_SIZE]

    def g_copy(h, i, j):
        return remote(gst.at[h, j], grecv.at[h, i], g_send.at[h, j], g_recv.at[h, i], j, t)

    def q_copy(h, m):
        return remote(
            qall.at[h, alpha], qall.at[h, alpha], q_send.at[h, m], q_recv.at[h, alpha],
            beta * a + m, t,
        )

    def w_copy(h, bb):
        return remote(
            wst.at[h, bb], wrecv.at[h, beta], w_send.at[h, bb], w_recv.at[h, beta],
            bb * a + alpha, t,
        )

    def score_own(o, h):
        k, _ = own_kv(o, h)
        s = dot_nt(k, q_s[...])
        parts = []
        for p in range(local):
            blk = o * local + p
            bias = row_bias([sel_ref[me * local + r, me * owner + blk] for r in range(local)])
            key = blk * KB + lax.broadcasted_iota(jnp.int32, (KB, wide), 0)
            parts.append(jnp.where(key <= lane, s[p * KB : (p + 1) * KB] + bias, NEG))
        return jnp.concatenate(parts, axis=0)

    def attend(h, wait_kv):
        for gr in range(group):
            hh = h * group + gr
            at = slice(gr * rows, (gr + 1) * rows)
            q_s[at, :] = (q_ref[:, head_cols(hh)].astype(F32) * scale).astype(BF16)
            g_s[at, :] = g_ref[:, head_cols(hh)]
        m = jnp.full((1, wide), NEG, F32)
        for o in range(own_chunks):
            s = score_own(o, h)
            s_buf[o] = s
            m = jnp.maximum(m, jnp.max(s, axis=0, keepdims=True))

        def pass_a(j, m):
            if wait_kv:
                kv_copy(j, j).wait_recv()
            picks = slots(me, j)
            s = dot_nt(far_k(j, h), q_s[...])
            parts = []
            for p in range(local):
                flags = []
                for r in range(local):
                    f = jnp.int32(0)
                    for blk in range(owner):
                        f = f + picks[p][blk] * sel_ref[me * local + r, j * owner + blk]
                    flags.append(f)
                parts.append(s[p * KB : (p + 1) * KB] + row_bias(flags))
            s = jnp.concatenate(parts, axis=0)
            s_buf[own_chunks + j] = s
            return jnp.maximum(m, jnp.max(s, axis=0, keepdims=True))

        m = lax.fori_loop(0, me, pass_a, m)

        def pass_b(idx, v, l, rd):
            p = jnp.exp(s_buf[idx] - m)
            dp = dot_nt(v, g_s[...])
            s_buf[idx] = p
            dp_buf[idx] = dp
            return (
                l + jnp.sum(p, axis=0, keepdims=True),
                rd + jnp.sum(p * dp, axis=0, keepdims=True),
            )

        l = jnp.zeros((1, wide), F32)
        rd = jnp.zeros((1, wide), F32)
        for o in range(own_chunks):
            l, rd = pass_b(o, own_kv(o, h)[1], l, rd)
        l, rd = lax.fori_loop(
            0, me, lambda j, c: pass_b(own_chunks + j, far_v(j, h), c[0], c[1]), (l, rd)
        )
        inv = 1.0 / l
        rd = rd * inv

        def pass_c(idx, k):
            pn = s_buf[idx] * inv
            ds = (pn * (dp_buf[idx] - rd)).astype(BF16)
            dv = dot_nn(pn.astype(BF16), g_s[...])
            dk = dot_nn(ds, q_s[...])
            return dot_tn(ds, k), dk, dv

        def far_c(j, carry):
            dq, dk, dv = pass_c(own_chunks + j, far_k(j, h))
            gst[h, j, :, 0:HEAD_SIZE] = dk.astype(BF16)
            gst[h, j, :, HEAD_SIZE : 2 * HEAD_SIZE] = dv.astype(BF16)
            dq_acc[...] += dq
            g_copy(h, me, j).start()
            return carry

        for o in range(own_chunks):
            dq, dk, dv = pass_c(o, own_kv(o, h)[0])
            at = slice(o * chunk, (o + 1) * chunk)
            own_acc[h, at, 0:HEAD_SIZE] = dk
            own_acc[h, at, HEAD_SIZE : 2 * HEAD_SIZE] = dv
            if o == 0:
                dq_acc[...] = dq
            else:
                dq_acc[...] += dq
        lax.fori_loop(0, me, far_c, 0)
        for gr in range(group):
            part = (dq_acc[gr * rows : (gr + 1) * rows, :] * scale).astype(BF16)
            dq_ref[:, head_cols(h * group + gr)] = part
            qall[h, alpha, :, head_cols(gr)] = part
        for mm in range(a):

            @pl.when(alpha != mm)
            def _():
                q_copy(h, mm).start()

    def weight_part(h, wait_x):
        if wait_x:
            for m in range(a):
                for bb in range(b):
                    own = jnp.logical_and(alpha == m, lax.div(bb * a + alpha, n_chunk) == t)

                    @pl.when(jnp.logical_not(own))
                    def _():
                        remote(
                            xst.at[0], xbuf.at[m, bb], x_send.at[0, 0], x_recv.at[m, bb], me, t
                        ).wait_recv()

        for mm in range(a):

            @pl.when(alpha != mm)
            def _():
                remote(
                    qall.at[h, mm], qall.at[h, mm], q_send.at[h, mm], q_recv.at[h, mm], me, t
                ).wait_recv()

        def partial(bb):
            out = dot_tn(xbuf[0, bb], qall[h, 0])
            for m in range(1, a):
                out = out + dot_tn(xbuf[m, bb], qall[h, m])
            return out

        for d in range(1, b):
            bb = lax.rem(beta + d, b)
            wst[h, bb] = partial(bb).astype(BF16)
            w_copy(h, bb).start()
        w_own[h] = partial(beta)

    for h in range(heads):
        attend(h, h == 0)
    for h in range(heads):
        weight_part(h, h == 0)

    for h in range(heads):

        def add_far(i, carry):
            remote(gst.at[h, 0], grecv.at[h, i], g_send.at[h, 0], g_recv.at[h, i], me, t).wait_recv()
            picks = slots(i, me)
            for p in range(local):
                got = grecv[h, i, p * KB : (p + 1) * KB, :].astype(F32)
                for blk in range(owner):
                    own_acc[h, blk * KB : (blk + 1) * KB, :] += jnp.where(
                        picks[p][blk] > 0, got, 0.0
                    )
            return carry

        lax.fori_loop(me + 1, n, add_far, 0)
        dk_ref[:, head_cols(h)] = own_acc[h, :, 0:HEAD_SIZE].astype(BF16)
        dv_ref[:, head_cols(h)] = own_acc[h, :, HEAD_SIZE : 2 * HEAD_SIZE].astype(BF16)

    for h in range(heads):
        total = w_own[h]
        for d in range(1, b):
            bb = lax.rem(beta + d, b)
            remote(
                wst.at[h, bb], wrecv.at[h, bb], w_send.at[h, bb], w_recv.at[h, bb], me, t
            ).wait_recv()
            total = total + wrecv[h, bb].astype(F32)
        w_ref[:, h * gcols : (h + 1) * gcols] = total

    def done_kv(i, carry):
        kv_copy(i, me).wait_send()
        return carry

    lax.fori_loop(me + 1, n, done_kv, 0)
    for q in range(n_chunk):
        c = t * n_chunk + q
        for tt in range(tp):

            @pl.when(jnp.logical_not(jnp.logical_and(lax.rem(c, a) == alpha, t == tt)))
            def _():
                x_copy(q, tt).wait_send()

    for h in range(heads):

        def done_g(j, carry):
            g_copy(h, me, j).wait_send()
            return carry

        lax.fori_loop(0, me, done_g, 0)
        for mm in range(a):

            @pl.when(alpha != mm)
            def _():
                q_copy(h, mm).wait_send()

        for d in range(1, b):
            w_copy(h, lax.rem(beta + d, b)).wait_send()


def body(n, tp, inputs, queries, key_vectors, value_rows_by_head, out_grad, chosen):
    rows, cols = key_vectors.shape
    q_cols = queries.shape[1]
    heads = cols // HEAD_SIZE
    group = q_cols // cols
    local = rows // QB
    chunk = local * KB
    own_chunks = rows // chunk
    wide = group * rows
    d_model = inputs.shape[1] * tp
    width = d_model // n
    n_chunk = inputs.shape[1] // width
    a = 4
    b = n // a
    gcols = group * HEAD_SIZE
    blocks = n * rows // KB
    sel = jnp.any(
        chosen[:, :, None] == jnp.arange(blocks, dtype=jnp.int32)[None, None, :], axis=1
    ).astype(jnp.int32)
    vmem = pl.BlockSpec(memory_space=pltpu.VMEM)
    dma = pltpu.SemaphoreType.DMA
    return pl.pallas_call(
        functools.partial(kernel, n, tp, a, b),
        out_shape=(
            jax.ShapeDtypeStruct((rows, q_cols), BF16),
            jax.ShapeDtypeStruct((rows, cols), BF16),
            jax.ShapeDtypeStruct((rows, cols), BF16),
            jax.ShapeDtypeStruct((width, q_cols), F32),
        ),
        in_specs=[pl.BlockSpec(memory_space=pltpu.SMEM)] + [vmem] * 5,
        out_specs=(vmem,) * 4,
        scratch_shapes=[
            pltpu.VMEM((n, chunk, 2 * cols), BF16),
            pltpu.VMEM((n, chunk, 2 * cols), BF16),
            pltpu.VMEM((n_chunk, rows, width), BF16),
            pltpu.VMEM((a, b, rows, width), BF16),
            pltpu.VMEM((wide, HEAD_SIZE), BF16),
            pltpu.VMEM((wide, HEAD_SIZE), BF16),
            pltpu.VMEM((own_chunks + n - 1, chunk, wide), F32),
            pltpu.VMEM((own_chunks + n - 1, chunk, wide), F32),
            pltpu.VMEM((wide, HEAD_SIZE), F32),
            pltpu.VMEM((heads, n, chunk, 2 * HEAD_SIZE), BF16),
            pltpu.VMEM((heads, n, chunk, 2 * HEAD_SIZE), BF16),
            pltpu.VMEM((heads, rows, 2 * HEAD_SIZE), F32),
            pltpu.VMEM((heads, a, rows, gcols), BF16),
            pltpu.VMEM((heads, b, width, gcols), BF16),
            pltpu.VMEM((heads, b, width, gcols), BF16),
            pltpu.VMEM((heads, width, gcols), F32),
            dma((n,)),
            dma((n,)),
            dma((n_chunk, tp)),
            dma((a, b)),
            dma((heads, n)),
            dma((heads, n)),
            dma((heads, a)),
            dma((heads, a)),
            dma((heads, b)),
            dma((heads, b)),
        ],
        compiler_params=pltpu.CompilerParams(
            collective_id=0, has_side_effects=True, vmem_limit_bytes=60 * 1024 * 1024
        ),
    )(sel, inputs, queries, key_vectors, value_rows_by_head, out_grad)


def solution(mesh):
    n, tp = mesh.shape["kv"], mesh.shape["tp"]
    placed = (P("kv", "tp"),) * 5 + (P(),)
    return jax.shard_map(
        functools.partial(body, n, tp),
        mesh=mesh,
        in_specs=placed,
        out_specs=(P("kv", "tp"),) * 4,
        check_vma=False,
    )
```

profile of v0, /device:TPU:3, one launch (start us, length us, event | category | flops | bytes accessed | tf_op | source)
XLA Modules:
  0.0 60.5 jit_solution(156491135015090388)
XLA Ops:
  0.6 0.8 %fusion = pred[16,32]{1,0:T(8,128)(4,1)S(1)} fusion(s32[16,16]{1,0:T(8,128)} %param.11), kind=kLoop, calls=%fused_computation.1 | loop fusion | flops 15872 | bytes 1536 | tf_op jit(solution)/shard_map/reduce_or | solution.py:384
  1.4 0.6 %convert_element_type.3.sel_ref = s32[16,32]{1,0:T(8,128)} convert(pred[16,32]{1,0:T(8,128)(4,1)S(1)} %fusion) | non-fusion elementwise | flops 512 | bytes 2560 | tf_op jit(solution)/shard_map/convert_element_type | solution.py:386
  2.1 53.8 %shard_map.93 = (bf16[256,512]{1,0:T(8,128)(2,1)}, bf16[256,128]{1,0:T(8,128)(2,1)}, bf16[256,128]{1,0:T(8,128)(2,1)}, f32[256,512]{1,0:T(8,128)}) custom-call(s32[16,32]{1,0:T(8,128)} %convert_element_type.3.sel_ref, bf16[256,512]{1,0:T(8,128)(2,1)} %x_ref.1, bf16[256,512]{1,0:T(8,128)(2,1)} %q_ref.1, bf16[256,128]{1,0:T(8,128)(2,1)} %k_ref.1, ...), custom_call_target="tpu_custom_call" | custom-call | tf_op jit(solution)/shard_map/pallas_call | solution.py:389
  55.9 0.0 copy-start
  55.9 1.7 %copy.14 = bf16[256,512]{1,0:T(8,128)(2,1)} copy(bf16[256,512]{1,0:T(8,128)(2,1)} %get-tuple-element.8) | data formatting | bytes 524288
  57.6 0.0 copy-start.1
  57.6 1.5 %copy.15 = bf16[256,128]{1,0:T(8,128)(2,1)} copy(bf16[256,128]{1,0:T(8,128)(2,1)} %get-tuple-element.9) | data formatting | bytes 131072
  59.1 0.0 copy-done.1
  59.1 0.6 %copy.16 = bf16[256,128]{1,0:T(8,128)(2,1)} copy(bf16[256,128]{1,0:T(8,128)(2,1)S(1)} %copy-done.1) | data formatting | bytes 131072
  59.7 0.0 copy-done
  59.7 0.8 %copy.17 = f32[256,512]{1,0:T(8,128)} copy(f32[256,512]{1,0:T(8,128)S(1)} %copy-done) | data formatting | bytes 1048576
Async XLA Ops:
  55.9 3.9 %copy-start = (f32[256,512]{1,0:T(8,128)S(1)}, f32[256,512]{1,0:T(8,128)}, u32[]{:S(2)}) copy-start(f32[256,512]{1,0:T(8,128)} %get-tuple-element.11) | copy-start | bytes 1572868
  57.6 1.5 %copy-start.1 = (bf16[256,128]{1,0:T(8,128)(2,1)S(1)}, bf16[256,128]{1,0:T(8,128)(2,1)}, u32[]{:S(2)}) copy-start(bf16[256,128]{1,0:T(8,128)(2,1)} %get-tuple-element.10) | copy-start | bytes 196612
where the time goes:
time: 60.8 us; the launch traced here: 60.5 us
  Pallas kernels  53.8 us (88%)
  local copies, waits for them, and re-layouts  4.66 us (8%)
  other arithmetic  1.42 us (2%)
  between operations  0.65 us (1%)
    pallas_call x1, Pallas kernels, body(): pl.pallas_call(functools.partial(kernel, n, tp, a, b), out_shape=(jax.Sha...  53.8 us
    unnamed x8, local copies, waits for them, and re-layouts  4.66 us

commit v1 on v0

v1 whole, which is shorter than its diff:
```python
import functools

import jax
import jax.numpy as jnp
from jax import lax
from jax.experimental import pallas as pl
from jax.experimental.pallas import tpu as pltpu
from jax.sharding import PartitionSpec as P

HEAD_SIZE = 64
QB = 128
KB = 64
NEG = -1e30
BF16 = jnp.bfloat16
F32 = jnp.float32
MESH = pl.DeviceIdType.MESH


def dot_nt(x, y):
    return lax.dot_general(x, y, (((1,), (1,)), ((), ())), preferred_element_type=F32)


def dot_nn(x, y):
    return lax.dot_general(x, y, (((1,), (0,)), ((), ())), preferred_element_type=F32)


def dot_tn(x, y):
    return lax.dot_general(x, y, (((0,), (0,)), ((), ())), preferred_element_type=F32)


def kernel(
    n, tp, a, b,
    chosen_ref, x_ref, q_ref, k_ref, v_ref, g_ref,
    dq_ref, dk_ref, dv_ref, w_ref,
    ch_v, sel_v, sel_s, x_in, xst, q_in, g_in, k_in, v_in, qz, gz, kvown, kvst, kvbuf, xbuf,
    e_buf, dp_buf, mj_buf, dqt, gst, grecv, own_acc, qall, wst, wrecv, w_own,
    ld, kv_send, kv_recv, x_send, x_recv, f_send, g_send, g_recv, q_send, q_recv,
    w_send, w_recv,
):
    me = lax.axis_index("kv")
    t = lax.axis_index("tp")
    alpha = lax.rem(me, a)
    beta = lax.div(me, a)
    parity = lax.rem(t, 2)
    partner = t + 1 - 2 * parity
    rows, cols = k_in.shape
    heads = cols // HEAD_SIZE
    group = q_in.shape[1] // cols
    local = rows // QB
    owner = rows // KB
    chunk = local * KB
    wide = group * rows
    width = xst.shape[2]
    n_chunk = xst.shape[0]
    gcols = group * HEAD_SIZE
    scale = HEAD_SIZE ** (-0.5)
    single_at = rows
    pair_at = rows + chunk

    def remote(src, dst, send, recv, kv, tpi):
        return pltpu.make_async_remote_copy(
            src_ref=src, dst_ref=dst, send_sem=send, recv_sem=recv,
            device_id=(kv, tpi), device_id_type=MESH,
        )

    barrier = pltpu.get_barrier_semaphore()
    for d in range(1, n):
        pl.semaphore_signal(
            barrier, inc=1, device_id=(lax.rem(me + d, n), t), device_id_type=MESH
        )
    for d in range(2, tp, 2):
        for m in range(a):
            pl.semaphore_signal(
                barrier, inc=1, device_id=(beta * a + m, lax.rem(t + d, tp)),
                device_id_type=MESH,
            )
    pl.semaphore_signal(barrier, inc=1, device_id=(me, partner), device_id_type=MESH)

    loads = [
        pltpu.make_async_copy(src, dst, ld.at[i])
        for i, (src, dst) in enumerate(
            [(chosen_ref, ch_v), (k_ref, k_in), (v_ref, v_in), (q_ref, q_in), (g_ref, g_in)]
            + (
                [(x_ref, x_in)]
                if width % 128
                else [
                    (x_ref.at[:, q * width : (q + 1) * width], xst.at[q])
                    for q in range(n_chunk)
                ]
            )
        )
    ]
    for c in loads:
        c.start()

    loads[0].wait()
    picked = ch_v[...]
    ids = lax.broadcasted_iota(jnp.int32, sel_v.shape, 1)
    hit = jnp.zeros(sel_v.shape, jnp.int32)
    for s in range(picked.shape[1]):
        hit = jnp.where(picked[:, s : s + 1] == ids, 1, hit)
    sel_v[...] = hit
    to_scalar = pltpu.make_async_copy(sel_v, sel_s, ld.at[len(loads)])
    to_scalar.start()

    def head_cols(h):
        return slice(h * HEAD_SIZE, (h + 1) * HEAD_SIZE)

    loads[1].wait()
    loads[2].wait()
    for h in range(heads):
        for blk in range(owner):
            at = slice(blk * KB, (blk + 1) * KB)
            kvown[h, blk, :, 0:HEAD_SIZE] = k_in[at, head_cols(h)]
            kvown[h, blk, :, HEAD_SIZE : 2 * HEAD_SIZE] = v_in[at, head_cols(h)]
    to_scalar.wait()

    def used_blocks(i, j):
        used = []
        for blk in range(owner):
            u = sel_s[i * local, j * owner + blk]
            for r in range(1, local):
                u = jnp.maximum(u, sel_s[i * local + r, j * owner + blk])
            used.append(u)
        return used

    def slots(i, j):
        used = used_blocks(i, j)
        picks = []
        for p in range(local):
            before = jnp.int32(0)
            one = []
            for blk in range(owner):
                one.append(jnp.where(before == p, used[blk], 0))
                before = before + used[blk]
            picks.append(one)
        return picks

    def kv_copy(h, i, j):
        return remote(kvst.at[h, i], kvbuf.at[h, j], kv_send.at[h, i], kv_recv.at[h, j], i, t)

    def stage_kv(ii, carry):
        i = n - 1 - ii
        picks = slots(i, me)
        for p in range(local):
            at = jnp.int32(0)
            for blk in range(owner):
                at = at + picks[p][blk] * blk
            for h in range(heads):
                kvst[h, i, p * KB : (p + 1) * KB, :] = kvown[h, at]
        return carry

    lax.fori_loop(0, n - 1 - me, stage_kv, 0)

    pl.semaphore_wait(barrier, n + (tp // 2 - 1) * a)

    for h in range(heads):

        def start_kv(ii, carry):
            kv_copy(h, n - 1 - ii, me).start()
            return carry

        lax.fori_loop(0, n - 1 - me, start_kv, 0)

    for c in loads[5:]:
        c.wait()
    if width % 128:
        for q in range(n_chunk):
            xst[q] = x_in[:, q * width : (q + 1) * width]

    def x_copy(q, y):
        c = t * n_chunk + q
        return remote(
            xst.at[q], xbuf.at[alpha, lax.div(c, a)], x_send.at[q, y],
            x_recv.at[alpha, lax.div(c, a)], beta * a + lax.rem(c, a), 2 * y + parity,
        )

    def x_mine(q, y):
        return jnp.logical_and(lax.rem(t * n_chunk + q, a) == alpha, t == 2 * y + parity)

    for q in range(n_chunk):
        c = t * n_chunk + q
        for y in range(tp // 2):

            @pl.when(jnp.logical_not(x_mine(q, y)))
            def _():
                x_copy(q, y).start()

            @pl.when(x_mine(q, y))
            def _():
                xbuf[alpha, lax.div(c, a)] = xst[q]

    loads[3].wait()
    loads[4].wait()
    for h in range(heads):
        for gr in range(group):
            hh = h * group + gr
            at = slice(gr * rows, (gr + 1) * rows)
            qz[h, at, 0:HEAD_SIZE] = (q_in[:, head_cols(hh)].astype(F32) * scale).astype(BF16)
            qz[h, at, HEAD_SIZE : 2 * HEAD_SIZE] = jnp.zeros((rows, HEAD_SIZE), BF16)
            gz[h, at, 0:HEAD_SIZE] = jnp.zeros((rows, HEAD_SIZE), BF16)
            gz[h, at, HEAD_SIZE : 2 * HEAD_SIZE] = g_in[:, head_cols(hh)]

    lane = lax.broadcasted_iota(jnp.int32, (1, rows), 1)
    lane_block = lax.div(lane, QB)

    def row_bias(flags):
        vals = [jnp.where(f > 0, F32(0.0), F32(NEG)) for f in flags]
        out = jnp.full((1, rows), vals[0], F32)
        for r in range(1, local):
            out = jnp.where(lane_block == r, vals[r], out)
        return out

    def own_bias():
        return [
            row_bias([sel_s[me * local + r, me * owner + blk] for r in range(local)])
            for blk in range(owner)
        ]

    def far_bias(j):
        picks = slots(me, j)
        out = []
        for p in range(local):
            flags = []
            for r in range(local):
                f = jnp.int32(0)
                for blk in range(owner):
                    f = f + picks[p][blk] * sel_s[me * local + r, j * owner + blk]
                flags.append(f)
            out.append(row_bias(flags))
        return out

    def tile(gr):
        return slice(gr * rows, (gr + 1) * rows)

    def g_copy(h, i, j):
        return remote(gst.at[h, j], grecv.at[h, i], g_send.at[h, j], g_recv.at[h, i], j, t)

    def q_copy(h, m):
        return remote(
            qall.at[h, alpha], qall.at[h, alpha], q_send.at[h, m], q_recv.at[h, alpha],
            beta * a + m, t,
        )

    def w_copy(h, bb):
        return remote(
            wst.at[h, bb], wrecv.at[h, beta], w_send.at[h, bb], w_recv.at[h, beta],
            bb * a + alpha, t,
        )

    def first_pass(h, kv, base, idx, bias, causal, stats):
        size = kv.shape[0]
        out = []
        for gr in range(group):
            m, l, rd = stats[gr]
            s = dot_nt(kv, qz[h, tile(gr), :])
            parts = []
            for p in range(size // KB):
                part = s[p * KB : (p + 1) * KB] + bias[p]
                if causal:
                    key = p * KB + lax.broadcasted_iota(jnp.int32, (KB, rows), 0)
                    part = jnp.where(key <= lane, part, NEG)
                parts.append(part)
            s = jnp.concatenate(parts, axis=0)
            mj = jnp.maximum(m, jnp.max(s, axis=0, keepdims=True))
            e = jnp.exp(s - mj)
            dp = dot_nt(kv, gz[h, tile(gr), :])
            e_buf[pl.ds(base, size), tile(gr)] = e
            dp_buf[pl.ds(base, size), tile(gr)] = dp
            mj_buf[idx, :, tile(gr)] = mj
            back = jnp.exp(m - mj)
            l = l * back + jnp.sum(e, axis=0, keepdims=True)
            rd = rd * back + jnp.sum(e * dp, axis=0, keepdims=True)
            out.append((mj, l, rd))
        return tuple(out)

    def second_pass(h, kv, base, idx, stats, first):
        size = kv.shape[0]
        keys = kv[:, 0:HEAD_SIZE]
        out = None
        for gr in range(group):
            m, inv, rd = stats[gr]
            f = jnp.exp(mj_buf[idx, :, tile(gr)] - m) * inv
            p = e_buf[pl.ds(base, size), tile(gr)] * f
            ds = (p * (dp_buf[pl.ds(base, size), tile(gr)] - rd)).astype(BF16)
            term = dot_nn(ds, qz[h, tile(gr), :]) + dot_nn(p.astype(BF16), gz[h, tile(gr), :])
            out = term if out is None else out + term
            dq = dot_tn(keys, ds)
            if first:
                dqt[:, tile(gr)] = dq
            else:
                dqt[:, tile(gr)] += dq
        return out

    odd = lax.rem(me, 2)
    pairs = lax.div(me, 2)

    def own_kv(h):
        return jnp.concatenate([kvown[h, blk] for blk in range(owner)], axis=0)

    def pair_kv(h, jj):
        return jnp.concatenate([kvbuf[h, 2 * jj], kvbuf[h, 2 * jj + 1]], axis=0)

    def attend(h):
        none = jnp.full((1, rows), NEG, F32)
        zero = jnp.zeros((1, rows), F32)
        stats = first_pass(
            h, own_kv(h), 0, 0, own_bias(), True, ((none, zero, zero),) * group
        )

        def one_single(_, stats):
            j = me - 1
            kv_copy(h, j, j).wait_recv()
            return first_pass(h, kvbuf[h, j], single_at, 1, far_bias(j), False, stats)

        stats = lax.fori_loop(0, odd, one_single, stats)

        def one_pair(ii, stats):
            jj = pairs - 1 - ii
            for d in range(2):
                kv_copy(h, 2 * jj + d, 2 * jj + d).wait_recv()
            base = pl.multiple_of(pair_at + jj * (2 * chunk), chunk)
            bias = far_bias(2 * jj) + far_bias(2 * jj + 1)
            return first_pass(h, pair_kv(h, jj), base, 2 + jj, bias, False, stats)

        stats = lax.fori_loop(0, pairs, one_pair, stats)
        fin = []
        for m, l, rd in stats:
            inv = 1.0 / l
            fin.append((m, inv, rd * inv))

        own_acc[h] = second_pass(h, own_kv(h), 0, 0, fin, True)

        def back_pair(jj, carry):
            base = pl.multiple_of(pair_at + jj * (2 * chunk), chunk)
            out = second_pass(h, pair_kv(h, jj), base, 2 + jj, fin, False).astype(BF16)
            for d in range(2):
                gst[h, 2 * jj + d] = out[d * chunk : (d + 1) * chunk]
            for d in range(2):
                g_copy(h, me, 2 * jj + d).start()
            return carry

        lax.fori_loop(0, pairs, back_pair, 0)

        def back_single(_, carry):
            j = me - 1
            gst[h, j] = second_pass(h, kvbuf[h, j], single_at, 1, fin, False).astype(BF16)
            g_copy(h, me, j).start()
            return carry

        lax.fori_loop(0, odd, back_single, 0)

        stacked = jnp.concatenate([dqt[:, tile(gr)] for gr in range(group)], axis=0)
        part = (stacked * scale).T.astype(BF16)
        qall[h, alpha] = part
        dq_ref[:, h * gcols : (h + 1) * gcols] = part
        for mm in range(a):

            @pl.when(alpha != mm)
            def _():
                q_copy(h, mm).start()

    def x_direct(bb):
        return lax.rem(lax.div(bb * a + alpha, n_chunk), 2) == parity

    def x_at_home(m, bb):
        return jnp.logical_and(alpha == m, lax.div(bb * a + alpha, n_chunk) == t)

    def x_here(m, bb):
        return remote(
            xst.at[0], xbuf.at[m, bb], x_send.at[0, 0], x_recv.at[m, bb], me, t
        )

    def x_forward(m, bb):
        return remote(
            xbuf.at[m, bb], xbuf.at[m, bb], f_send.at[m, bb], x_recv.at[m, bb], me, partner
        )

    def relay_x():
        for bb in range(b):
            for m in range(a):

                @pl.when(x_direct(bb))
                def _():
                    @pl.when(jnp.logical_not(x_at_home(m, bb)))
                    def _():
                        x_here(m, bb).wait_recv()

                    x_forward(m, bb).start()

    def gather_x():
        for bb in range(b):
            for m in range(a):

                @pl.when(jnp.logical_not(x_direct(bb)))
                def _():
                    x_here(m, bb).wait_recv()

    def weight_part(h):
        for mm in range(a):

            @pl.when(alpha != mm)
            def _():
                remote(
                    qall.at[h, mm], qall.at[h, mm], q_send.at[h, mm], q_recv.at[h, mm], me, t
                ).wait_recv()

        def partial(bb):
            out = dot_tn(xbuf[0, bb], qall[h, 0])
            for m in range(1, a):
                out = out + dot_tn(xbuf[m, bb], qall[h, m])
            return out

        for d in range(1, b):
            bb = lax.rem(beta + d, b)
            wst[h, bb] = partial(bb).astype(BF16)
            w_copy(h, bb).start()
        w_own[h] = partial(beta)

    for h in range(heads):
        attend(h)
        if h == 0:
            relay_x()
    gather_x()
    for h in range(heads):
        weight_part(h)

    for h in range(heads):

        def add_far(i, carry):
            remote(gst.at[h, 0], grecv.at[h, i], g_send.at[h, 0], g_recv.at[h, i], me, t).wait_recv()
            picks = slots(i, me)
            for p in range(local):
                got = grecv[h, i, p * KB : (p + 1) * KB, :].astype(F32)
                for blk in range(owner):
                    own_acc[h, blk * KB : (blk + 1) * KB, :] += jnp.where(
                        picks[p][blk] > 0, got, 0.0
                    )
            return carry

        lax.fori_loop(me + 1, n, add_far, 0)
        dk_ref[:, head_cols(h)] = own_acc[h, :, 0:HEAD_SIZE].astype(BF16)
        dv_ref[:, head_cols(h)] = own_acc[h, :, HEAD_SIZE : 2 * HEAD_SIZE].astype(BF16)

    for h in range(heads):
        total = w_own[h]
        for d in range(1, b):
            bb = lax.rem(beta + d, b)
            remote(
                wst.at[h, bb], wrecv.at[h, bb], w_send.at[h, bb], w_recv.at[h, bb], me, t
            ).wait_recv()
            total = total + wrecv[h, bb].astype(F32)
        w_ref[:, h * gcols : (h + 1) * gcols] = total

    for h in range(heads):

        def done_kv(i, carry):
            kv_copy(h, i, me).wait_send()
            return carry

        lax.fori_loop(me + 1, n, done_kv, 0)
    for q in range(n_chunk):
        for y in range(tp // 2):

            @pl.when(jnp.logical_not(x_mine(q, y)))
            def _():
                x_copy(q, y).wait_send()

    for bb in range(b):
        for m in range(a):

            @pl.when(x_direct(bb))
            def _():
                x_forward(m, bb).wait_send()

    for h in range(heads):

        def done_g(j, carry):
            g_copy(h, me, j).wait_send()
            return carry

        lax.fori_loop(0, me, done_g, 0)
        for mm in range(a):

            @pl.when(alpha != mm)
            def _():
                q_copy(h, mm).wait_send()

        for d in range(1, b):
            w_copy(h, lax.rem(beta + d, b)).wait_send()


def write_out(*refs):
    count = (len(refs) - 1) // 2
    sems = refs[-1]
    copies = [
        pltpu.make_async_copy(refs[i], refs[count + i], sems.at[i]) for i in range(count)
    ]
    for c in copies:
        c.start()
    for c in copies:
        c.wait()


def body(n, tp, inputs, queries, key_vectors, value_rows_by_head, out_grad, chosen):
    rows, cols = key_vectors.shape
    q_cols = queries.shape[1]
    heads = cols // HEAD_SIZE
    group = q_cols // cols
    local = rows // QB
    chunk = local * KB
    wide = group * rows
    d_model = inputs.shape[1] * tp
    width = d_model // n
    n_chunk = inputs.shape[1] // width
    a = 4
    b = n // a
    gcols = group * HEAD_SIZE
    blocks = n * rows // KB
    lanes = -(-blocks // 128) * 128
    keys = rows + chunk + (n // 2) * 2 * chunk
    vmem = pl.BlockSpec(memory_space=pltpu.VMEM)
    hbm = pl.BlockSpec(memory_space=pl.ANY)
    dma = pltpu.SemaphoreType.DMA
    outs = (
        ((rows, q_cols), BF16),
        ((rows, cols), BF16),
        ((rows, cols), BF16),
        ((width, q_cols), F32),
    )
    held = pl.pallas_call(
        functools.partial(kernel, n, tp, a, b),
        out_shape=tuple(pltpu.VMEM(s, d) for s, d in outs),
        in_specs=[hbm] * 6,
        out_specs=(vmem,) * 4,
        scratch_shapes=[
            pltpu.VMEM(chosen.shape, jnp.int32),
            pltpu.VMEM((chosen.shape[0], lanes), jnp.int32),
            pltpu.SMEM((chosen.shape[0], lanes), jnp.int32),
            pltpu.VMEM(inputs.shape, BF16),
            pltpu.VMEM((n_chunk, rows, width), BF16),
            pltpu.VMEM((rows, q_cols), BF16),
            pltpu.VMEM((rows, q_cols), BF16),
            pltpu.VMEM((rows, cols), BF16),
            pltpu.VMEM((rows, cols), BF16),
            pltpu.VMEM((heads, wide, 2 * HEAD_SIZE), BF16),
            pltpu.VMEM((heads, wide, 2 * HEAD_SIZE), BF16),
            pltpu.VMEM((heads, rows // KB, KB, 2 * HEAD_SIZE), BF16),
            pltpu.VMEM((heads, n, chunk, 2 * HEAD_SIZE), BF16),
            pltpu.VMEM((heads, n, chunk, 2 * HEAD_SIZE), BF16),
            pltpu.VMEM((a, b, rows, width), BF16),
            pltpu.VMEM((keys, wide), F32),
            pltpu.VMEM((keys, wide), F32),
            pltpu.VMEM((2 + n // 2, 1, wide), F32),
            pltpu.VMEM((HEAD_SIZE, wide), F32),
            pltpu.VMEM((heads, n, chunk, 2 * HEAD_SIZE), BF16),
            pltpu.VMEM((heads, n, chunk, 2 * HEAD_SIZE), BF16),
            pltpu.VMEM((heads, rows, 2 * HEAD_SIZE), F32),
            pltpu.VMEM((heads, a, rows, gcols), BF16),
            pltpu.VMEM((heads, b, width, gcols), BF16),
            pltpu.VMEM((heads, b, width, gcols), BF16),
            pltpu.VMEM((heads, width, gcols), F32),
            dma((6 + n_chunk,)),
            dma((heads, n)),
            dma((heads, n)),
            dma((n_chunk, tp // 2)),
            dma((a, b)),
            dma((a, b)),
            dma((heads, n)),
            dma((heads, n)),
            dma((heads, a)),
            dma((heads, a)),
            dma((heads, b)),
            dma((heads, b)),
        ],
        compiler_params=pltpu.CompilerParams(
            collective_id=0, has_side_effects=True, vmem_limit_bytes=58 * 1024 * 1024
        ),
    )(chosen, inputs, queries, key_vectors, value_rows_by_head, out_grad)
    return pl.pallas_call(
        write_out,
        out_shape=tuple(jax.ShapeDtypeStruct(s, d) for s, d in outs),
        in_specs=[vmem] * 4,
        out_specs=(hbm,) * 4,
        scratch_shapes=[dma((4,))],
        compiler_params=pltpu.CompilerParams(vmem_limit_bytes=1024 * 1024),
    )(*held)


def solution(mesh):
    n, tp = mesh.shape["kv"], mesh.shape["tp"]
    placed = (P("kv", "tp"),) * 5 + (P(),)
    return jax.shard_map(
        functools.partial(body, n, tp),
        mesh=mesh,
        in_specs=placed,
        out_specs=(P("kv", "tp"),) * 4,
        check_vma=False,
    )
```

time: 60.8 us -> 47.1 us (0.77)
  the two profiles are of different devices: /device:TPU:3 before, /device:TPU:2 now
where the time goes in v1:
time: 47.1 us; the launch traced here: 46.9 us
  Pallas kernels  46.2 us (98%)
  between operations  0.64 us (1%)
    pallas_call x1, Pallas kernels, body(): pl.pallas_call(functools.partial(kernel, n, tp, a, b), out_shape=tuple((p...  45.3 us
    pallas_call x1, Pallas kernels, body(): pl.pallas_call(write_out, out_shape=tuple((jax.ShapeDtypeStruct(s, d) for...  0.96 us

profile of v1, /device:TPU:2, one launch (start us, length us, event | category | flops | bytes accessed | tf_op | source)
XLA Modules:
  0.0 46.9 jit_solution(15815229194717310542)
XLA Ops:
  0.6 45.3 %shard_map.93 = (bf16[256,512]{1,0:T(8,128)(2,1)S(1)}, bf16[256,128]{1,0:T(8,128)(2,1)S(1)}, bf16[256,128]{1,0:T(8,128)(2,1)S(1)}, f32[256,512]{1,0:T(8,128)S(1)}) custom-call(s32[16,16]{1,0:T(8,128)} %chosen_ref.1, bf16[256,512]{1,0:T(8,128)(2,1)} %x_ref.1, bf16[256,512]{1,0:T(8,128)(2,1)} %q_ref.1, bf16[256,128]{1,0:T(8,128)(2,1)} %k_ref.1, ...), custom_call_target="tpu_custom_call" | custom-call | tf_op jit(solution)/shard_map/pallas_call | solution.py:531
  45.9 1.0 %shard_map.94 = (bf16[256,512]{1,0:T(8,128)(2,1)}, bf16[256,128]{1,0:T(8,128)(2,1)}, bf16[256,128]{1,0:T(8,128)(2,1)}, f32[256,512]{1,0:T(8,128)}) custom-call(bf16[256,512]{1,0:T(8,128)(2,1)S(1)} %get-tuple-element.8.refs_0_, bf16[256,128]{1,0:T(8,128)(2,1)S(1)} %get-tuple-element.9.refs_1_, bf16[256,128]{1,0:T(8,128)(2,1)S(1)} %get-tuple-element.10.refs_2_, ...), custom_call_target="tpu_custom_call" | custom-call | tf_op jit(solution)/shard_map/pallas_call | solution.py:580

commit v2 on v1

--- a/solution.py
+++ b/solution.py
@@ -11,6 +11,7 @@
 QB = 128
 KB = 64
 NEG = -1e30
+PARTS = 2
 BF16 = jnp.bfloat16
 F32 = jnp.float32
 MESH = pl.DeviceIdType.MESH
@@ -32,10 +33,10 @@
     n, tp, a, b,
     chosen_ref, x_ref, q_ref, k_ref, v_ref, g_ref,
     dq_ref, dk_ref, dv_ref, w_ref,
-    ch_v, sel_v, sel_s, x_in, xst, q_in, g_in, k_in, v_in, qz, gz, kvown, kvst, kvbuf, xbuf,
+    ch_v, sel_v, sel_s, x_in, xst, q_in, g_in, k_in, v_in, qz, gz, kvown, kvst, kvbuf, xbuf, xt,
     e_buf, dp_buf, mj_buf, dqt, gst, grecv, own_acc, qall, wst, wrecv, w_own,
     ld, kv_send, kv_recv, x_send, x_recv, f_send, g_send, g_recv, q_send, q_recv,
-    w_send, w_recv,
+    w_send, w_recv, pair_sem,
 ):
     me = lax.axis_index("kv")
     t = lax.axis_index("tp")
@@ -43,6 +44,13 @@
     beta = lax.div(me, a)
     parity = lax.rem(t, 2)
     partner = t + 1 - 2 * parity
+
+    def flip(m, step):
+        for bit in (1, 2):
+            if step & bit:
+                m = m + bit - 2 * bit * lax.rem(lax.div(m, bit), 2)
+        return m
+
     rows, cols = k_in.shape
     heads = cols // HEAD_SIZE
     group = q_in.shape[1] // cols
@@ -52,10 +60,11 @@
     wide = group * rows
     width = xst.shape[2]
     n_chunk = xst.shape[0]
-    gcols = group * HEAD_SIZE
+    parts = qall.shape[0] // heads
+    ucols = qall.shape[3]
     scale = HEAD_SIZE ** (-0.5)
-    single_at = rows
-    pair_at = rows + chunk
+    single_at = heads * rows
+    pair_at = single_at + chunk
 
     def remote(src, dst, send, recv, kv, tpi):
         return pltpu.make_async_remote_copy(
@@ -69,11 +78,9 @@
             barrier, inc=1, device_id=(lax.rem(me + d, n), t), device_id_type=MESH
         )
     for d in range(2, tp, 2):
-        for m in range(a):
-            pl.semaphore_signal(
-                barrier, inc=1, device_id=(beta * a + m, lax.rem(t + d, tp)),
-                device_id_type=MESH,
-            )
+        pl.semaphore_signal(
+            barrier, inc=1, device_id=(me, lax.rem(t + d, tp)), device_id_type=MESH
+        )
     pl.semaphore_signal(barrier, inc=1, device_id=(me, partner), device_id_type=MESH)
 
     loads = [
@@ -152,15 +159,16 @@
 
     lax.fori_loop(0, n - 1 - me, stage_kv, 0)
 
-    pl.semaphore_wait(barrier, n + (tp // 2 - 1) * a)
-
-    for h in range(heads):
-
+    pl.semaphore_wait(barrier, n + tp // 2 - 1)
+
+    def send_kv(h):
         def start_kv(ii, carry):
             kv_copy(h, n - 1 - ii, me).start()
             return carry
 
         lax.fori_loop(0, n - 1 - me, start_kv, 0)
+
+    send_kv(0)
 
     for c in loads[5:]:
         c.wait()
@@ -168,27 +176,27 @@
         for q in range(n_chunk):
             xst[q] = x_in[:, q * width : (q + 1) * width]
 
-    def x_copy(q, y):
+    def x_copy(q):
         c = t * n_chunk + q
         return remote(
-            xst.at[q], xbuf.at[alpha, lax.div(c, a)], x_send.at[q, y],
-            x_recv.at[alpha, lax.div(c, a)], beta * a + lax.rem(c, a), 2 * y + parity,
-        )
-
-    def x_mine(q, y):
-        return jnp.logical_and(lax.rem(t * n_chunk + q, a) == alpha, t == 2 * y + parity)
-
-    for q in range(n_chunk):
-        c = t * n_chunk + q
-        for y in range(tp // 2):
-
-            @pl.when(jnp.logical_not(x_mine(q, y)))
+            xst.at[q], xbuf.at[alpha, lax.div(c, a)], x_send.at[q],
+            x_recv.at[alpha, lax.div(c, a)], beta * a + lax.rem(c, a), t,
+        )
+
+    def send_x(late):
+        for q in range(n_chunk):
+            c = t * n_chunk + q
+            ahead = lax.rem(c, a) - alpha
+
+            @pl.when(ahead > 1 if late else jnp.logical_and(ahead < 2, ahead != 0))
             def _():
-                x_copy(q, y).start()
-
-            @pl.when(x_mine(q, y))
-            def _():
-                xbuf[alpha, lax.div(c, a)] = xst[q]
+                x_copy(q).start()
+
+            if not late:
+
+                @pl.when(ahead == 0)
+                def _():
+                    xbuf[alpha, lax.div(c, a)] = xst[q]
 
     loads[3].wait()
     loads[4].wait()
@@ -236,11 +244,23 @@
     def g_copy(h, i, j):
         return remote(gst.at[h, j], grecv.at[h, i], g_send.at[h, j], g_recv.at[h, i], j, t)
 
-    def q_copy(h, m):
+    def hop(u):
+        return 1 + u % 2
+
+    def q_send_to(h, m, step):
+        own = m is alpha
         return remote(
-            qall.at[h, alpha], qall.at[h, alpha], q_send.at[h, m], q_recv.at[h, alpha],
-            beta * a + m, t,
-        )
+            qall.at[h, m], qall.at[h, m], q_send.at[h, step if own else 0], q_recv.at[h, m],
+            beta * a + flip(alpha, step), t,
+        )
+
+    def q_here(h, m):
+        return remote(qall.at[h, m], qall.at[h, m], q_send.at[h, 0], q_recv.at[h, m], me, t)
+
+    def relay_q(u):
+        m = flip(alpha, 3 - hop(u))
+        q_here(u, m).wait_recv()
+        q_send_to(u, m, hop(u)).start()
 
     def w_copy(h, bb):
         return remote(
@@ -254,14 +274,14 @@
         for gr in range(group):
             m, l, rd = stats[gr]
             s = dot_nt(kv, qz[h, tile(gr), :])
-            parts = []
+            rows_of = []
             for p in range(size // KB):
                 part = s[p * KB : (p + 1) * KB] + bias[p]
                 if causal:
                     key = p * KB + lax.broadcasted_iota(jnp.int32, (KB, rows), 0)
                     part = jnp.where(key <= lane, part, NEG)
-                parts.append(part)
-            s = jnp.concatenate(parts, axis=0)
+                rows_of.append(part)
+            s = jnp.concatenate(rows_of, axis=0)
             mj = jnp.maximum(m, jnp.max(s, axis=0, keepdims=True))
             e = jnp.exp(s - mj)
             dp = dot_nt(kv, gz[h, tile(gr), :])
@@ -301,18 +321,22 @@
     def pair_kv(h, jj):
         return jnp.concatenate([kvbuf[h, 2 * jj], kvbuf[h, 2 * jj + 1]], axis=0)
 
-    def attend(h):
+    state = {}
+
+    def own(h):
         none = jnp.full((1, rows), NEG, F32)
         zero = jnp.zeros((1, rows), F32)
-        stats = first_pass(
-            h, own_kv(h), 0, 0, own_bias(), True, ((none, zero, zero),) * group
-        )
-
+        state[h] = first_pass(
+            h, own_kv(h), h * rows, h, own_bias(), True, ((none, zero, zero),) * group
+        )
+
+    def far(h):
         def one_single(_, stats):
             j = me - 1
             kv_copy(h, j, j).wait_recv()
-            return first_pass(h, kvbuf[h, j], single_at, 1, far_bias(j), False, stats)
-
+            return first_pass(h, kvbuf[h, j], single_at, heads, far_bias(j), False, stats)
+
+        stats = state[h]
         stats = lax.fori_loop(0, odd, one_single, stats)
 
         def one_pair(ii, stats):
@@ -321,94 +345,111 @@
                 kv_copy(h, 2 * jj + d, 2 * jj + d).wait_recv()
             base = pl.multiple_of(pair_at + jj * (2 * chunk), chunk)
             bias = far_bias(2 * jj) + far_bias(2 * jj + 1)
-            return first_pass(h, pair_kv(h, jj), base, 2 + jj, bias, False, stats)
+            return first_pass(h, pair_kv(h, jj), base, heads + 1 + jj, bias, False, stats)
 
         stats = lax.fori_loop(0, pairs, one_pair, stats)
         fin = []
         for m, l, rd in stats:
             inv = 1.0 / l
             fin.append((m, inv, rd * inv))
-
-        own_acc[h] = second_pass(h, own_kv(h), 0, 0, fin, True)
+        state[h] = fin
+
+    def back(h):
+        fin = state[h]
+        own_acc[h] = second_pass(h, own_kv(h), h * rows, h, fin, True)
 
         def back_pair(jj, carry):
             base = pl.multiple_of(pair_at + jj * (2 * chunk), chunk)
-            out = second_pass(h, pair_kv(h, jj), base, 2 + jj, fin, False).astype(BF16)
+            out = second_pass(h, pair_kv(h, jj), base, heads + 1 + jj, fin, False).astype(BF16)
             for d in range(2):
                 gst[h, 2 * jj + d] = out[d * chunk : (d + 1) * chunk]
-            for d in range(2):
-                g_copy(h, me, 2 * jj + d).start()
             return carry
 
         lax.fori_loop(0, pairs, back_pair, 0)
 
         def back_single(_, carry):
             j = me - 1
-            gst[h, j] = second_pass(h, kvbuf[h, j], single_at, 1, fin, False).astype(BF16)
+            gst[h, j] = second_pass(h, kvbuf[h, j], single_at, heads, fin, False).astype(BF16)
+            return carry
+
+        lax.fori_loop(0, odd, back_single, 0)
+
+        per = group // parts
+        for u in range(parts):
+            stacked = jnp.concatenate(
+                [dqt[:, tile(gr)] for gr in range(u * per, (u + 1) * per)], axis=0
+            )
+            part = (stacked * scale).T.astype(BF16)
+            at = h * parts + u
+            qall[at, alpha] = part
+            dq_ref[:, at * ucols : (at + 1) * ucols] = part
+            for step in (2, 1):
+                q_send_to(at, alpha, step).start()
+
+    def send_g(h):
+        def start_g(j, carry):
             g_copy(h, me, j).start()
             return carry
 
-        lax.fori_loop(0, odd, back_single, 0)
-
-        stacked = jnp.concatenate([dqt[:, tile(gr)] for gr in range(group)], axis=0)
-        part = (stacked * scale).T.astype(BF16)
-        qall[h, alpha] = part
-        dq_ref[:, h * gcols : (h + 1) * gcols] = part
-        for mm in range(a):
-
-            @pl.when(alpha != mm)
+        lax.fori_loop(0, me, start_g, 0)
+
+    def x_source(bb):
+        return lax.div(bb * a + alpha, n_chunk)
+
+    def x_here(m, bb):
+        return remote(xst.at[0], xbuf.at[m, bb], x_send.at[0], x_recv.at[m, bb], me, t)
+
+    def x_forward(m, bb, d):
+        to = partner if d == 0 else lax.rem(t + 2 * d, tp)
+        return remote(
+            xbuf.at[m, bb], xbuf.at[m, bb], f_send.at[m, bb, d], x_recv.at[m, bb], me, to
+        )
+
+    def relay_x(step):
+        m = flip(alpha, step)
+        for bb in range(b):
+
+            @pl.when(x_source(bb) == t)
             def _():
-                q_copy(h, mm).start()
-
-    def x_direct(bb):
-        return lax.rem(lax.div(bb * a + alpha, n_chunk), 2) == parity
-
-    def x_at_home(m, bb):
-        return jnp.logical_and(alpha == m, lax.div(bb * a + alpha, n_chunk) == t)
-
-    def x_here(m, bb):
-        return remote(
-            xst.at[0], xbuf.at[m, bb], x_send.at[0, 0], x_recv.at[m, bb], me, t
-        )
-
-    def x_forward(m, bb):
-        return remote(
-            xbuf.at[m, bb], xbuf.at[m, bb], f_send.at[m, bb], x_recv.at[m, bb], me, partner
-        )
-
-    def relay_x():
+                if step:
+                    x_here(m, bb).wait_recv()
+                for d in range(tp // 2 - 1, -1, -1):
+                    x_forward(m, bb, d).start()
+
+    def relay_far(early):
+        lower = lax.rem(lax.div(alpha, 2), 2) == 0
+
+        @pl.when(lower if early else jnp.logical_not(lower))
+        def _():
+            relay_x(2)
+            relay_x(3)
+
+    def gather_x():
+        for step in range(a):
+            m = flip(alpha, step)
+            for bb in range(b):
+                src = x_source(bb)
+
+                @pl.when(src != t)
+                def _():
+                    x_here(m, bb).wait_recv()
+
+                @pl.when(jnp.logical_and(src != t, lax.rem(src, 2) == parity))
+                def _():
+                    x_forward(m, bb, 0).start()
+
         for bb in range(b):
             for m in range(a):
-
-                @pl.when(x_direct(bb))
-                def _():
-                    @pl.when(jnp.logical_not(x_at_home(m, bb)))
-                    def _():
-                        x_here(m, bb).wait_recv()
-
-                    x_forward(m, bb).start()
-
-    def gather_x():
-        for bb in range(b):
-            for m in range(a):
-
-                @pl.when(jnp.logical_not(x_direct(bb)))
-                def _():
-                    x_here(m, bb).wait_recv()
+                xt[m, bb] = xbuf[m, bb].T
 
     def weight_part(h):
-        for mm in range(a):
-
-            @pl.when(alpha != mm)
-            def _():
-                remote(
-                    qall.at[h, mm], qall.at[h, mm], q_send.at[h, mm], q_recv.at[h, mm], me, t
-                ).wait_recv()
+        q_here(h, flip(alpha, hop(h))).wait_recv()
+        q_here(h, flip(alpha, 3)).wait_recv()
 
         def partial(bb):
-            out = dot_tn(xbuf[0, bb], qall[h, 0])
+            out = dot_nn(xt[0, bb], qall[h, 0])
             for m in range(1, a):
-                out = out + dot_tn(xbuf[m, bb], qall[h, m])
+                out = out + dot_nn(xt[m, bb], qall[h, m])
             return out
 
         for d in range(1, b):
@@ -417,13 +458,46 @@
             w_copy(h, bb).start()
         w_own[h] = partial(beta)
 
-    for h in range(heads):
-        attend(h)
-        if h == 0:
-            relay_x()
+    def wait_kv(h):
+        def done_kv(i, carry):
+            kv_copy(h, i, me).wait_send()
+            return carry
+
+        lax.fori_loop(me + 1, n, done_kv, 0)
+
+    own(0)
+    wait_kv(0)
+    pl.semaphore_signal(pair_sem, inc=1, device_id=(me, partner), device_id_type=MESH)
+    if heads > 1:
+        own(1)
+    pl.semaphore_wait(pair_sem, 1)
+    for h in range(1, heads):
+        send_kv(h)
+    send_x(False)
+    far(0)
+    back(0)
+    send_g(0)
+    send_x(True)
+    relay_x(0)
+    relay_x(1)
+    relay_far(True)
+    for h in range(1, heads):
+        if h > 1:
+            own(h)
+        far(h)
+        for u in range((h - 1) * parts, h * parts):
+            relay_q(u)
+        back(h)
+        send_g(h)
+    relay_far(False)
     gather_x()
-    for h in range(heads):
-        weight_part(h)
+    last = (heads - 1) * parts
+    for u in range(last):
+        weight_part(u)
+    for u in range(last, heads * parts):
+        relay_q(u)
+    for u in range(last, heads * parts):
+        weight_part(u)
 
     for h in range(heads):
 
@@ -442,7 +516,7 @@
         dk_ref[:, head_cols(h)] = own_acc[h, :, 0:HEAD_SIZE].astype(BF16)
         dv_ref[:, head_cols(h)] = own_acc[h, :, HEAD_SIZE : 2 * HEAD_SIZE].astype(BF16)
 
-    for h in range(heads):
+    def wait_w(h):
         total = w_own[h]
         for d in range(1, b):
             bb = lax.rem(beta + d, b)
@@ -450,28 +524,31 @@
                 wst.at[h, bb], wrecv.at[h, bb], w_send.at[h, bb], w_recv.at[h, bb], me, t
             ).wait_recv()
             total = total + wrecv[h, bb].astype(F32)
-        w_ref[:, h * gcols : (h + 1) * gcols] = total
-
-    for h in range(heads):
-
-        def done_kv(i, carry):
-            kv_copy(h, i, me).wait_send()
-            return carry
-
-        lax.fori_loop(me + 1, n, done_kv, 0)
+        w_ref[:, h * ucols : (h + 1) * ucols] = total
+
+    for h in range(heads * parts):
+        wait_w(h)
+
+    for h in range(1, heads):
+        wait_kv(h)
     for q in range(n_chunk):
-        for y in range(tp // 2):
-
-            @pl.when(jnp.logical_not(x_mine(q, y)))
+
+        @pl.when(lax.rem(t * n_chunk + q, a) != alpha)
+        def _():
+            x_copy(q).wait_send()
+
+    for bb in range(b):
+        src = x_source(bb)
+        for m in range(a):
+
+            @pl.when(lax.rem(src, 2) == parity)
             def _():
-                x_copy(q, y).wait_send()
-
-    for bb in range(b):
-        for m in range(a):
-
-            @pl.when(x_direct(bb))
+                x_forward(m, bb, 0).wait_send()
+
+            @pl.when(src == t)
             def _():
-                x_forward(m, bb).wait_send()
+                for d in range(1, tp // 2):
+                    x_forward(m, bb, d).wait_send()
 
     for h in range(heads):
 
@@ -480,14 +557,13 @@
             return carry
 
         lax.fori_loop(0, me, done_g, 0)
-        for mm in range(a):
-
-            @pl.when(alpha != mm)
-            def _():
-                q_copy(h, mm).wait_send()
-
+
+    for u in range(heads * parts):
+        for step in (2, 1):
+            q_send_to(u, alpha, step).wait_send()
+        q_send_to(u, flip(alpha, 3 - hop(u)), hop(u)).wait_send()
         for d in range(1, b):
-            w_copy(h, lax.rem(beta + d, b)).wait_send()
+            w_copy(u, lax.rem(beta + d, b)).wait_send()
 
 
 def write_out(*refs):
@@ -515,10 +591,11 @@
     n_chunk = inputs.shape[1] // width
     a = 4
     b = n // a
-    gcols = group * HEAD_SIZE
+    units = heads * PARTS
+    ucols = group * HEAD_SIZE // PARTS
     blocks = n * rows // KB
     lanes = -(-blocks // 128) * 128
-    keys = rows + chunk + (n // 2) * 2 * chunk
+    keys = heads * rows + chunk + (n // 2) * 2 * chunk
     vmem = pl.BlockSpec(memory_space=pltpu.VMEM)
     hbm = pl.BlockSpec(memory_space=pl.ANY)
     dma = pltpu.SemaphoreType.DMA
@@ -549,29 +626,31 @@
             pltpu.VMEM((heads, n, chunk, 2 * HEAD_SIZE), BF16),
             pltpu.VMEM((heads, n, chunk, 2 * HEAD_SIZE), BF16),
             pltpu.VMEM((a, b, rows, width), BF16),
+            pltpu.VMEM((a, b, width, rows), BF16),
             pltpu.VMEM((keys, wide), F32),
             pltpu.VMEM((keys, wide), F32),
-            pltpu.VMEM((2 + n // 2, 1, wide), F32),
+            pltpu.VMEM((heads + 1 + n // 2, 1, wide), F32),
             pltpu.VMEM((HEAD_SIZE, wide), F32),
             pltpu.VMEM((heads, n, chunk, 2 * HEAD_SIZE), BF16),
             pltpu.VMEM((heads, n, chunk, 2 * HEAD_SIZE), BF16),
             pltpu.VMEM((heads, rows, 2 * HEAD_SIZE), F32),
-            pltpu.VMEM((heads, a, rows, gcols), BF16),
-            pltpu.VMEM((heads, b, width, gcols), BF16),
-            pltpu.VMEM((heads, b, width, gcols), BF16),
-            pltpu.VMEM((heads, width, gcols), F32),
+            pltpu.VMEM((units, a, rows, ucols), BF16),
+            pltpu.VMEM((units, b, width, ucols), BF16),
+            pltpu.VMEM((units, b, width, ucols), BF16),
+            pltpu.VMEM((units, width, ucols), F32),
             dma((6 + n_chunk,)),
             dma((heads, n)),
             dma((heads, n)),
-            dma((n_chunk, tp // 2)),
+            dma((n_chunk,)),
             dma((a, b)),
-            dma((a, b)),
+            dma((a, b, tp // 2)),
             dma((heads, n)),
             dma((heads, n)),
-            dma((heads, a)),
-            dma((heads, a)),
-            dma((heads, b)),
-            dma((heads, b)),
+            dma((units, a)),
+            dma((units, a)),
+            dma((units, b)),
+            dma((units, b)),
+            pltpu.SemaphoreType.REGULAR,
         ],
         compiler_params=pltpu.CompilerParams(
             collective_id=0, has_side_effects=True, vmem_limit_bytes=58 * 1024 * 1024

time: 47.1 us -> 43.7 us (0.928)
  the two profiles are of different devices: /device:TPU:2 before, /device:TPU:0 now
where the time goes in v2:
time: 43.7 us; the launch traced here: 43.5 us
  Pallas kernels  42.9 us (98%)
  between operations  0.64 us (1%)
    pallas_call x1, Pallas kernels, body(): pl.pallas_call(functools.partial(kernel, n, tp, a, b), out_shape=tuple((p...  41.9 us
    pallas_call x1, Pallas kernels, body(): pl.pallas_call(write_out, out_shape=tuple((jax.ShapeDtypeStruct(s, d) for...  0.96 us

profile of v2, /device:TPU:0, one launch (start us, length us, event | category | flops | bytes accessed | tf_op | source)
XLA Modules:
  0.0 43.5 jit_solution(13549576192850264616)
XLA Ops:
  0.6 41.9 %shard_map.93 = (bf16[256,512]{1,0:T(8,128)(2,1)S(1)}, bf16[256,128]{1,0:T(8,128)(2,1)S(1)}, bf16[256,128]{1,0:T(8,128)(2,1)S(1)}, f32[256,512]{1,0:T(8,128)S(1)}) custom-call(s32[16,16]{1,0:T(8,128)} %chosen_ref.1, bf16[256,512]{1,0:T(8,128)(2,1)} %x_ref.1, bf16[256,512]{1,0:T(8,128)(2,1)} %q_ref.1, bf16[256,128]{1,0:T(8,128)(2,1)} %k_ref.1, ...), custom_call_target="tpu_custom_call" | custom-call | tf_op jit(solution)/shard_map/pallas_call | solution.py:608
  42.6 1.0 %shard_map.94 = (bf16[256,512]{1,0:T(8,128)(2,1)}, bf16[256,128]{1,0:T(8,128)(2,1)}, bf16[256,128]{1,0:T(8,128)(2,1)}, f32[256,512]{1,0:T(8,128)}) custom-call(bf16[256,512]{1,0:T(8,128)(2,1)S(1)} %get-tuple-element.8.refs_0_, bf16[256,128]{1,0:T(8,128)(2,1)S(1)} %get-tuple-element.9.refs_1_, bf16[256,128]{1,0:T(8,128)(2,1)S(1)} %get-tuple-element.10.refs_2_, ...), custom_call_target="tpu_custom_call" | custom-call | tf_op jit(solution)/shard_map/pallas_call | solution.py:659

commit v3 on v2

--- a/solution.py
+++ b/solution.py
@@ -183,20 +183,29 @@
             x_recv.at[alpha, lax.div(c, a)], beta * a + lax.rem(c, a), t,
         )
 
-    def send_x(late):
+    def send_x(way):
         for q in range(n_chunk):
             c = t * n_chunk + q
-            ahead = lax.rem(c, a) - alpha
-
-            @pl.when(ahead > 1 if late else jnp.logical_and(ahead < 2, ahead != 0))
+            to = lax.rem(c, a)
+            rise = lax.div(to, 2) - lax.div(alpha, 2)
+            if way < 0:
+                due = rise < 0
+            elif way > 0:
+                due = rise > 0
+            else:
+                due = jnp.logical_and(rise == 0, to != alpha)
+
+            @pl.when(due)
             def _():
                 x_copy(q).start()
 
-            if not late:
-
-                @pl.when(ahead == 0)
+            if way == 0:
+
+                @pl.when(to == alpha)
                 def _():
                     xbuf[alpha, lax.div(c, a)] = xst[q]
+
+    send_x(-1)
 
     loads[3].wait()
     loads[4].wait()
@@ -356,13 +365,15 @@
 
     def back(h):
         fin = state[h]
-        own_acc[h] = second_pass(h, own_kv(h), h * rows, h, fin, True)
+        dqt[...] = jnp.zeros_like(dqt)
 
         def back_pair(jj, carry):
             base = pl.multiple_of(pair_at + jj * (2 * chunk), chunk)
             out = second_pass(h, pair_kv(h, jj), base, heads + 1 + jj, fin, False).astype(BF16)
             for d in range(2):
                 gst[h, 2 * jj + d] = out[d * chunk : (d + 1) * chunk]
+            for d in range(2):
+                g_copy(h, me, 2 * jj + d).start()
             return carry
 
         lax.fori_loop(0, pairs, back_pair, 0)
@@ -370,9 +381,11 @@
         def back_single(_, carry):
             j = me - 1
             gst[h, j] = second_pass(h, kvbuf[h, j], single_at, heads, fin, False).astype(BF16)
+            g_copy(h, me, j).start()
             return carry
 
         lax.fori_loop(0, odd, back_single, 0)
+        own_acc[h] = second_pass(h, own_kv(h), h * rows, h, fin, False)
 
         per = group // parts
         for u in range(parts):
@@ -473,11 +486,10 @@
     pl.semaphore_wait(pair_sem, 1)
     for h in range(1, heads):
         send_kv(h)
-    send_x(False)
+    send_x(0)
     far(0)
     back(0)
-    send_g(0)
-    send_x(True)
+    send_x(1)
     relay_x(0)
     relay_x(1)
     relay_far(True)
@@ -488,7 +500,6 @@
         for u in range((h - 1) * parts, h * parts):
             relay_q(u)
         back(h)
-        send_g(h)
     relay_far(False)
     gather_x()
     last = (heads - 1) * parts

time: 43.7 us -> 42 us (0.961)
  Pallas kernels: 42.9 us -> 41.2 us
    pallas_call x1, Pallas kernels: 41.9 us -> 40.2 us  [body(): pl.pallas_call(functools.partial(kernel, n, tp, a, b), out_shape=tuple((p...]
where the time goes in v3:
time: 42 us; the launch traced here: 41.8 us
  Pallas kernels  41.2 us (98%)
  between operations  0.64 us (2%)
    pallas_call x1, Pallas kernels, body(): pl.pallas_call(functools.partial(kernel, n, tp, a, b), out_shape=tuple((p...  40.2 us
    pallas_call x1, Pallas kernels, body(): pl.pallas_call(write_out, out_shape=tuple((jax.ShapeDtypeStruct(s, d) for...  0.96 us

profile of v3, /device:TPU:0, one launch (start us, length us, event | category | flops | bytes accessed | tf_op | source)
XLA Modules:
  0.0 41.8 jit_solution(8278905302360738199)
XLA Ops:
  0.6 40.2 %shard_map.93 = (bf16[256,512]{1,0:T(8,128)(2,1)S(1)}, bf16[256,128]{1,0:T(8,128)(2,1)S(1)}, bf16[256,128]{1,0:T(8,128)(2,1)S(1)}, f32[256,512]{1,0:T(8,128)S(1)}) custom-call(s32[16,16]{1,0:T(8,128)} %chosen_ref.1, bf16[256,512]{1,0:T(8,128)(2,1)} %x_ref.1, bf16[256,512]{1,0:T(8,128)(2,1)} %q_ref.1, bf16[256,128]{1,0:T(8,128)(2,1)} %k_ref.1, ...), custom_call_target="tpu_custom_call" | custom-call | tf_op jit(solution)/shard_map/pallas_call | solution.py:619
  40.9 1.0 %shard_map.94 = (bf16[256,512]{1,0:T(8,128)(2,1)}, bf16[256,128]{1,0:T(8,128)(2,1)}, bf16[256,128]{1,0:T(8,128)(2,1)}, f32[256,512]{1,0:T(8,128)}) custom-call(bf16[256,512]{1,0:T(8,128)(2,1)S(1)} %get-tuple-element.8.refs_0_, bf16[256,128]{1,0:T(8,128)(2,1)S(1)} %get-tuple-element.9.refs_1_, bf16[256,128]{1,0:T(8,128)(2,1)S(1)} %get-tuple-element.10.refs_2_, ...), custom_call_target="tpu_custom_call" | custom-call | tf_op jit(solution)/shard_map/pallas_call | solution.py:670

commit v4 on v3

--- a/solution.py
+++ b/solution.py
@@ -396,7 +396,7 @@
             at = h * parts + u
             qall[at, alpha] = part
             dq_ref[:, at * ucols : (at + 1) * ucols] = part
-            for step in (2, 1):
+            for step in (1, 2):
                 q_send_to(at, alpha, step).start()
 
     def send_g(h):
@@ -469,7 +469,6 @@
             bb = lax.rem(beta + d, b)
             wst[h, bb] = partial(bb).astype(BF16)
             w_copy(h, bb).start()
-        w_own[h] = partial(beta)
 
     def wait_kv(h):
         def done_kv(i, carry):
@@ -489,8 +488,8 @@
     send_x(0)
     far(0)
     back(0)
+    relay_x(0)
     send_x(1)
-    relay_x(0)
     relay_x(1)
     relay_far(True)
     for h in range(1, heads):
@@ -509,6 +508,15 @@
         relay_q(u)
     for u in range(last, heads * parts):
         weight_part(u)
+
+    def own_part(h, bb):
+        out = dot_nn(xt[0, bb], qall[h, 0])
+        for m in range(1, a):
+            out = out + dot_nn(xt[m, bb], qall[h, m])
+        return out
+
+    for h in range(heads * parts):
+        w_own[h] = own_part(h, beta)
 
     for h in range(heads):
 

time: 42 us -> 41.9 us (level)
  no operation moved by 1% of the time
where the time goes in v4:
time: 41.9 us; the launch traced here: 41.7 us
  Pallas kernels  41 us (98%)
  between operations  0.64 us (2%)
    pallas_call x1, Pallas kernels, body(): pl.pallas_call(functools.partial(kernel, n, tp, a, b), out_shape=tuple((p...  40.1 us
    pallas_call x1, Pallas kernels, body(): pl.pallas_call(write_out, out_shape=tuple((jax.ShapeDtypeStruct(s, d) for...  0.96 us

profile of v4, /device:TPU:0, one launch (start us, length us, event | category | flops | bytes accessed | tf_op | source)
XLA Modules:
  0.0 41.7 jit_solution(442194070506592251)
XLA Ops:
  0.6 40.1 %shard_map.93 = (bf16[256,512]{1,0:T(8,128)(2,1)S(1)}, bf16[256,128]{1,0:T(8,128)(2,1)S(1)}, bf16[256,128]{1,0:T(8,128)(2,1)S(1)}, f32[256,512]{1,0:T(8,128)S(1)}) custom-call(s32[16,16]{1,0:T(8,128)} %chosen_ref.1, bf16[256,512]{1,0:T(8,128)(2,1)} %x_ref.1, bf16[256,512]{1,0:T(8,128)(2,1)} %q_ref.1, bf16[256,128]{1,0:T(8,128)(2,1)} %k_ref.1, ...), custom_call_target="tpu_custom_call" | custom-call | tf_op jit(solution)/shard_map/pallas_call | solution.py:627
  40.7 1.0 %shard_map.94 = (bf16[256,512]{1,0:T(8,128)(2,1)}, bf16[256,128]{1,0:T(8,128)(2,1)}, bf16[256,128]{1,0:T(8,128)(2,1)}, f32[256,512]{1,0:T(8,128)}) custom-call(bf16[256,512]{1,0:T(8,128)(2,1)S(1)} %get-tuple-element.8.refs_0_, bf16[256,128]{1,0:T(8,128)(2,1)S(1)} %get-tuple-element.9.refs_1_, bf16[256,128]{1,0:T(8,128)(2,1)S(1)} %get-tuple-element.10.refs_2_, ...), custom_call_target="tpu_custom_call" | custom-call | tf_op jit(solution)/shard_map/pallas_call | solution.py:678
